TPU v7x, 32 devices: a whole 2x2x4 slice. The times are simulated.
32 devices in a mesh: grp: 2 (over y), sp: 4 (over z), tp: 4 (over x, core).
Axes of the slice: x: 2, y: 2, z: 4, core: 2. Of those that a mesh axis runs over, the one named last changes fastest.
Arguments:
- query_rows: bfloat16 [1024, 1024], P(('grp', 'sp'), 'tp'), parts along dimension 0, may hold values from -6 to 6
- key_rows: bfloat16 [1024, 1024], P(('grp', 'sp'), 'tp'), parts along dimension 0, may hold values from -6 to 6
- value_rows: bfloat16 [1024, 1024], P(('grp', 'sp'), 'tp'), parts along dimension 0, may hold values from -6 to 6
- gate_rows: bfloat16 [1024, 1024], P(('grp', 'sp'), 'tp'), parts along dimension 0, may hold values from -6 to 6
- log_decay: float32 [2, 8, 1024], P(None, 'tp', ('grp', 'sp')), parts along dimension 2, may hold values from -2 to 0, as said below
- head_gain: float32 [2, 1024], P(None, 'tp'), may hold values from 0.1 to 1.9
- out_weight: bfloat16 [1024, 2048], P('tp'), may hold values from -0.1875 to 0.1875
- residual: bfloat16 [1024, 2048], P(('grp', 'sp')), parts along dimension 0, may hold values from -6 to 6
- norm_gain: bfloat16 [2048], replicated, may hold values from 0.099609375 to 1.8984375
- gate_weight: bfloat16 [2048, 5632], P('sp', 'tp'), may hold values from -0.125 to 0.125
- up_weight: bfloat16 [2048, 5632], P('sp', 'tp'), may hold values from -0.125 to 0.125
- down_weight: bfloat16 [2048, 5632], P('sp', 'tp'), may hold values from -0.078125 to 0.078125
- gate_taps: bfloat16 [3, 5632], P(None, 'tp'), may hold values from -3.5 to 3.5
- up_taps: bfloat16 [3, 5632], P(None, 'tp'), may hold values from -3.5 to 3.5
Outputs:
- block_out: bfloat16 [1024, 2048], P(('grp', 'sp', 'tp')), parts along dimension 0
There are 2 independent parts, one for each index of `grp`. A program takes and returns all parts, laid end to end along the dimension named above; an argument that names none is the same for every part. Nothing has to cross between parts.
Inputs may be any that keep to these rules, and one draw needn't show every extreme that they name: `log_decay`: every entry is negative.
All inputs are finite; a program needn't handle non-finite values.
Results may differ from a plain program's by a relative error of at most 0.017.
Values may be sent and summed in bfloat16 or wider, within the bound.
A program may use at most 64 MiB of HBM per device.

v0:
```python
import math
import jax
import jax.numpy as jnp
from jax import lax
from jax.sharding import PartitionSpec as P

HEAD = 128
FULL_PRECISION = lax.Precision.HIGHEST
GROUP_EPS = 1e-05
NORM_EPS = 1e-06


def prefix(value, axis, join, neutral, backward):
    count, mine = (lax.axis_size(axis), lax.axis_index(axis))
    pieces = jax.tree.map(lambda part: lax.all_gather(part, axis), value)
    if backward:
        pieces = jax.tree.map(lambda part: part[::-1], pieces)
        mine = count - 1 - mine
    running = jax.tree.map(
        lambda part, zero: jnp.full_like(part, 0) + jnp.asarray(zero, part.dtype), value, neutral
    )

    def lap(position, running):
        longer = join(running, jax.tree.map(lambda part: part[position], pieces))
        return jax.tree.map(lambda new, old: jnp.where(position < mine, new, old), longer, running)

    return lax.fori_loop(0, count - 1, lap, running)


def padded_2(shard, sides, width):
    for axis, dim in sides:
        size, length = (lax.axis_size(axis), shard.shape[dim])
        up = [(i, (i + 1) % size) for i in range(size - 1)]
        down = [(j, i) for i, j in up]
        last = lax.slice_in_dim(shard, length - width, length, axis=dim)
        initial = lax.slice_in_dim(shard, 0, width, axis=dim)
        before = lax.ppermute(last, axis, up)
        after = lax.ppermute(initial, axis, down)
        shard = jnp.concatenate([before, shard, after], axis=dim)
    return shard


def state_combine(earlier, later):
    return (earlier[0] * later[0], earlier[1] * later[0][:, None, None] + later[1])


def group_norm(values):
    length, head_count, head_width = values.shape
    centre = values - jnp.mean(values, axis=2, keepdims=True)
    spread = jnp.mean(centre * centre, axis=2, keepdims=True)
    return (centre * lax.rsqrt(spread + GROUP_EPS)).reshape(length, head_count * head_width)


def rms_scale(middle, gain):
    values = middle.astype(jnp.float32)
    multiplier = lax.rsqrt(jnp.mean(values * values, axis=1, keepdims=True) + NORM_EPS)
    return (values * multiplier * gain.astype(jnp.float32)).astype(jnp.bfloat16)


def local_retention(query_all, key_all, value_all, log_rates):
    length, head_count, head_width = query_all.shape
    block_len = math.gcd(length, 512)
    block_count = length // block_len
    cumul = jnp.cumsum(log_rates, axis=1).T
    query_block = query_all.reshape(block_count, block_len, head_count, head_width)
    key_block = key_all.reshape(block_count, block_len, head_count, head_width)
    value_block = value_all.reshape(block_count, block_len, head_count, head_width)
    cumul_block = cumul.reshape(block_count, block_len, head_count)
    before = jnp.concatenate(
        [jnp.zeros((1, head_count), jnp.float32), cumul_block[:-1, -1]], axis=0
    )
    local_cumul = cumul_block - before[:, None, :]
    gap_logs = local_cumul[:, :, None, :] - local_cumul[:, None, :, :]
    lower_mask = (jnp.arange(block_len)[:, None] >= jnp.arange(block_len)[None, :])[
        None, :, :, None
    ]
    decay_mask = jnp.where(lower_mask, jnp.exp(jnp.minimum(gap_logs, 0.0)), 0.0)
    scores = (
        jnp.einsum("bthd,bshd->btsh", query_block, key_block, precision=FULL_PRECISION) * decay_mask
    )
    inner_part = jnp.einsum("btsh,bshe->bthe", scores, value_block, precision=FULL_PRECISION)
    to_end = jnp.exp(local_cumul[:, -1:, :] - local_cumul)
    block_states = jnp.einsum(
        "bshd,bshe->bhde", key_block * to_end[..., None], value_block, precision=FULL_PRECISION
    )
    block_decay = jnp.exp(local_cumul[:, -1, :])

    def carry_step(carry_state, inputs):
        return (carry_state * inputs[0][:, None, None] + inputs[1], carry_state)

    zero_state = jnp.zeros((head_count, head_width, head_width), jnp.float32)
    end_state, entering = lax.scan(carry_step, zero_state, (block_decay, block_states))
    carried = jnp.einsum(
        "bthd,bhde->bthe",
        query_block * jnp.exp(local_cumul)[..., None],
        entering,
        precision=FULL_PRECISION,
    )
    output = (inner_part + carried).reshape(length, head_count, head_width)
    return (output, end_state, cumul, jnp.exp(cumul[-1]))


def with_incoming(output, query_all, cumul, incoming):
    return output + jnp.einsum(
        "thd,hde->the", query_all * jnp.exp(cumul)[:, :, None], incoming, precision=FULL_PRECISION
    )


def shards(
    query_rows,
    key_rows,
    value_rows,
    gate_rows,
    log_decay,
    head_gain,
    out_weight,
    residual,
    norm_gain,
    gate_weight,
    up_weight,
    down_weight,
    gate_taps,
    up_taps,
):
    pair_local = jnp.concatenate([gate_weight, up_weight], axis=1)
    row_count = query_rows.shape[0]
    head_count = query_rows.shape[1] // HEAD
    key_scale = HEAD ** (-0.5)
    query_all = query_rows.astype(jnp.float32).reshape(row_count, head_count, HEAD)
    key_all = key_rows.astype(jnp.float32).reshape(row_count, head_count, HEAD) * key_scale
    value_all = value_rows.astype(jnp.float32).reshape(row_count, head_count, HEAD)
    identity = (
        jnp.ones((head_count,), jnp.float32),
        jnp.zeros((head_count, HEAD, HEAD), jnp.float32),
    )
    ahead_local, ahead_state, ahead_cumul, ahead_decay = local_retention(
        query_all, key_all, value_all, log_decay[0]
    )
    query_back = query_all[::-1]
    behind_local, behind_state, behind_cumul, behind_decay = local_retention(
        query_back, key_all[::-1], value_all[::-1], log_decay[1][:, ::-1]
    )
    ahead_in = prefix((ahead_decay, ahead_state), "sp", state_combine, identity, False)[1]
    behind_in = prefix((behind_decay, behind_state), "sp", state_combine, identity, True)[1]
    ahead_out = with_incoming(ahead_local, query_all, ahead_cumul, ahead_in)
    behind_out = with_incoming(behind_local, query_back, behind_cumul, behind_in)[::-1]
    combined = group_norm(ahead_out) * head_gain[0] + group_norm(behind_out) * head_gain[1]
    mixed_heads = (jax.nn.silu(gate_rows.astype(jnp.float32)) * combined).astype(jnp.bfloat16)
    gathered = (
        lax.all_gather(pair_local, "sp", axis=0, tiled=True),
        lax.all_gather(down_weight, "sp", axis=0, tiled=True),
    )
    pair_full, down_full = gathered
    share_rows = row_count // lax.axis_size("tp")
    own_start = lax.axis_index("tp") * share_rows
    picked = mixed_heads
    attended = lax.psum_scatter(
        jnp.dot(picked, out_weight, preferred_element_type=jnp.float32).astype(jnp.bfloat16),
        "tp",
        scatter_dimension=0,
        tiled=True,
    ).astype(jnp.float32)
    residual_own = lax.dynamic_slice_in_dim(residual, own_start, share_rows, 0)
    middle_own = lax.optimization_barrier(
        (residual_own.astype(jnp.float32) + attended).astype(jnp.bfloat16)
    )
    normed = rms_scale(middle_own, norm_gain)
    pre_both = jnp.dot(
        lax.all_gather(normed, "tp", axis=0, tiled=True),
        pair_full,
        preferred_element_type=jnp.float32,
    ).astype(jnp.bfloat16)
    padded = padded_2(pre_both, (("sp", 0),), 1)
    half_width = gate_taps.shape[1]
    tap_table = jnp.concatenate([gate_taps, up_taps], axis=1).astype(jnp.float32)
    conv_out = (
        tap_table[0] * padded[:-2].astype(jnp.float32)
        + tap_table[1] * padded[1:-1].astype(jnp.float32)
        + tap_table[2] * padded[2:].astype(jnp.float32)
    )
    hidden = (jax.nn.silu(conv_out[:, :half_width]) * conv_out[:, half_width:]).astype(jnp.bfloat16)
    picked = hidden
    ff_out = lax.psum_scatter(
        lax.dot_general(
            picked, down_full, (((1,), (1,)), ((), ())), preferred_element_type=jnp.float32
        ).astype(jnp.bfloat16),
        "tp",
        scatter_dimension=0,
        tiled=True,
    ).astype(jnp.float32)
    return (middle_own.astype(jnp.float32) + ff_out).astype(jnp.bfloat16)


def solution(mesh):
    in_specs = (
        P(("grp", "sp"), "tp"),
        P(("grp", "sp"), "tp"),
        P(("grp", "sp"), "tp"),
        P(("grp", "sp"), "tp"),
        P(None, "tp", ("grp", "sp")),
        P(None, "tp"),
        P("tp", None),
        P(("grp", "sp"), None),
        P(),
        P("sp", "tp"),
        P("sp", "tp"),
        P("sp", "tp"),
        P(None, "tp"),
        P(None, "tp"),
    )
    out_specs = P(("grp", "sp", "tp"), None)
    return jax.shard_map(shards, mesh=mesh, in_specs=in_specs, out_specs=out_specs, check_vma=False)
```

profile of v0, /device:TPU:0, one launch (start us, length us, event | category | flops | bytes accessed | tf_op | source)
XLA Modules:
  0.0 416.1 jit_solution(4977097718532471524)
XLA Ops:
  7.4 0.8 slice_bitcast_fusion.1
  8.2 0.3 reduce_window_sum.17
  8.5 0.2 slice_reduce_fusion.1
  8.8 0.1 rev.23
  8.9 0.3 reduce_window_sum.18
  9.2 0.2 slice_reduce_fusion
  9.4 1.0 copy.89
  10.4 0.2 reverse.3
  10.6 0.9 bitcast_convert_fusion
  11.5 1.0 convolution_add_fusion
  12.5 17.5 %all-gather = f32[8,128,128]{2,1,0:T(8,128)S(1)} all-gather(f32[2,128,128]{2,1,0:T(8,128)S(1)} %convolution_add_fusion), channel_id=2, replica_groups=mesh['grp'=2,'sp'=4,'tp'=4] {'sp'}, dimensions={0}, use_global_device_ids=true | all-gather | bytes 655360 | tf_op jit(solution)/shard_map/all_gather | solution.py:15
  30.0 0.2 exponential_reduce_fusion.1
  30.2 11.7 %all-gather.2 = f32[4,1,2]{2,1,0:T(1,128)S(1)} all-gather(f32[1,1,2]{2,1,0:T(1,128)S(1)} %bitcast.179), channel_id=1, replica_groups=mesh['grp'=2,'sp'=4,'tp'=4] {'sp'}, dimensions={0}, use_global_device_ids=true | all-gather | bytes 40 | tf_op jit(solution)/shard_map/all_gather | solution.py:15
  41.9 0.4 while.18
  41.9 0.1 fusion.84
  42.0 0.1 fusion.84
  42.2 0.1 fusion.84
  42.3 0.5 fusion.33
  42.7 0.4 convolution_bitcast_fusion.3
  43.2 0.3 fusion.9
  43.5 0.3 fusion.62
  43.8 0.1 rev.24
  43.9 0.3 convolution_add_fusion.1
  44.2 15.1 %all-gather.1 = f32[8,128,128]{2,1,0:T(8,128)S(1)} all-gather(f32[2,128,128]{2,1,0:T(8,128)S(1)} %convolution_add_fusion.1), channel_id=3, replica_groups=mesh['grp'=2,'sp'=4,'tp'=4] {'sp'}, dimensions={0}, use_global_device_ids=true | all-gather | bytes 655360 | tf_op jit(solution)/shard_map/all_gather | solution.py:15
  59.4 0.2 exponential_reduce_fusion
  59.6 8.0 %all-gather.3 = f32[4,1,2]{2,1,0:T(1,128)S(1)} all-gather(f32[1,1,2]{2,1,0:T(1,128)S(1)} %bitcast.180), channel_id=1, replica_groups=mesh['grp'=2,'sp'=4,'tp'=4] {'sp'}, dimensions={0}, use_global_device_ids=true | all-gather | bytes 40 | tf_op jit(solution)/shard_map/all_gather | solution.py:15
  67.6 0.1 copy.75
  67.7 0.1 rev.25
  67.8 0.1 copy.76
  67.9 0.4 while.19
  67.9 0.1 fusion.85
  68.0 0.1 fusion.85
  68.1 0.1 fusion.85
  68.2 0.1 rev.22
  68.3 0.4 fusion.11
  68.7 0.3 fusion.30
  69.0 0.3 convolution_bitcast_fusion
  69.4 0.4 fusion.7
  69.8 0.1 rev.27
  69.8 0.1 reduce_sum.47
  70.0 0.2 multiply_reduce_fusion
  70.2 0.1 subtract_multiply_fusion
  70.3 0.1 copy.79
  70.5 0.1 copy.58
  70.6 0.1 fusion.28
  70.7 1.1 convolution_convert_fusion.1
  72.0 3.1 pad_maximum_fusion
  75.2 0.5 all-gather.9.cloned.1.call-update
  75.8 17.1 %reduce-scatter.3.cloned.1.call-done = bf16[32,2048]{1,0:T(8,128)(2,1)} async-done(((bf16[128,2048]{1,0:T(8,128)(2,1)}), bf16[32,2048]{1,0:T(8,128)(2,1)}) %reduce-scatter.3.cloned.1.call-update) | async-done | bytes 131088 | tf_op jit(solution)/shard_map/reduce_scatter | solution.py:157
  92.9 1.0 add_convert_fusion
  93.9 0.1 fusion.15
  94.1 0.1 fusion.17
  94.2 6.6 %all_gather.29 = bf16[128,2048]{1,0:T(8,128)(2,1)S(1)} all-gather(bf16[32,2048]{1,0:T(8,128)(2,1)S(1)} %fusion.17), channel_id=1, replica_groups=mesh['grp'=2,'sp'=4,'tp'=4] {'tp'}, dimensions={0}, use_global_device_ids=true | all-gather | bytes 655360 | tf_op jit(solution)/shard_map/all_gather | solution.py:169
  100.8 174.5 %all-gather.7.cloned.1.call-done = bf16[2048,2816]{1,0:T(8,128)(2,1)} async-done(((bf16[512,2816]{1,0:T(8,128)(2,1)}), bf16[2048,2816]{1,0:T(8,128)(2,1)}) %all-gather.7.cloned.1.call-update) | async-done | bytes 11534352 | tf_op jit(solution)/shard_map/all_gather | solution.py:150
  275.3 5.9 %convolution_convert_fusion = bf16[128,2816]{1,0:T(8,128)(2,1)S(1)} fusion(bf16[128,2048]{1,0:T(8,128)(2,1)S(1)} %all_gather.29, bf16[2048,2816]{1,0:T(8,128)(2,1)} %all-gather.7.cloned.1.call-done), kind=kOutput, calls=%fused_computation.6 | convolution fusion | flops 1476755456 | bytes 12779520 | tf_op jit(solution)/shard_map/dot_general | solution.py:168
  281.3 1.3 collective-permute-start
  282.6 1.3 collective-permute-start.1
  283.9 0.1 convert_reduce_fusion.1
  284.1 4.6 %collective-permute-done.1 = bf16[1,2816]{1,0:T(2,128)(2,1)S(1)} collective-permute-done((bf16[1,2816]{1,0:T(2,128)(2,1)S(1)}, bf16[1,2816]{1,0:T(2,128)(2,1)S(1)}, u32[]{:S(2)}, u32[]{:S(2)}) %collective-permute-start.1) | collective-permute-done | bytes 5664 | tf_op jit(solution)/shard_map/ppermute | solution.py:38
  288.7 0.5 multiply_add_fusion
  289.2 92.5 %all-gather.9.cloned.1.call-done = bf16[2048,1408]{1,0:T(8,128)(2,1)} async-done(((bf16[512,1408]{1,0:T(8,128)(2,1)}), bf16[2048,1408]{1,0:T(8,128)(2,1)}) %all-gather.9.cloned.1.call-update) | async-done | bytes 5767184 | tf_op jit(solution)/shard_map/all_gather | solution.py:151
  381.7 5.4 %convolution_convert_fusion.2 = bf16[128,2048]{1,0:T(8,128)(2,1)} fusion(bf16[2048,1408]{1,0:T(8,128)(2,1)} %all-gather.9.cloned.1.call-done, f32[128,2816]{1,0:T(8,128)S(1)} %multiply_add_fusion), kind=kOutput, calls=%fused_computation.9 | convolution fusion | flops 739540992 | bytes 7733248 | tf_op jit(solution)/shard_map/dot_general | solution.py:184
  387.1 20.0 %reduce-scatter.5.cloned.1.call-done = bf16[32,2048]{1,0:T(8,128)(2,1)} async-done(((bf16[128,2048]{1,0:T(8,128)(2,1)}), bf16[32,2048]{1,0:T(8,128)(2,1)}) %reduce-scatter.5.cloned.1.call-update) | async-done | bytes 131088 | tf_op jit(solution)/shard_map/reduce_scatter | solution.py:183
  407.1 1.6 fusion.18
  (51 shorter events, 0.6 us)
Async XLA Ops:
  7.4 63.4 %copy-start = (bf16[256,2048]{1,0:T(8,128)(2,1)S(1)}, bf16[256,2048]{1,0:T(8,128)(2,1)}, u32[]{:S(2)}) copy-start(bf16[256,2048]{1,0:T(8,128)(2,1)} %param.24) | copy-start | bytes 3145732
  7.4 85.6 %reduce-scatter.3.cloned.1.call-start = ((), (), s32[]{:S(2)}) async-start(), calls=%async_computation.2 | async-start | bytes 655360 | tf_op jit(solution)/shard_map/reduce_scatter | solution.py:157
  12.5 29.7 %copy-start.2 = (bf16[128,256]{1,0:T(8,128)(2,1)S(1)}, bf16[128,256]{1,0:T(8,128)(2,1)}, u32[]{:S(2)}) copy-start(bf16[128,256]{1,0:T(8,128)(2,1)} %param.18) | copy-start | bytes 196612
  41.9 1.6 copy-start.3
  68.3 2.1 copy-start.8
  68.3 2.1 copy-start.4
  70.3 1.6 copy-start.1
  71.9 203.4 %all-gather.7.cloned.1.call-start = ((), (), s32[]{:S(2)}) async-start(), calls=%async_computation.3 | async-start | bytes 14417920 | tf_op jit(solution)/shard_map/all_gather | solution.py:150
  75.1 0.7 copy-start.7
  75.1 306.6 %all-gather.9.cloned.1.call-start = ((), (), s32[]{:S(2)}) async-start(), calls=%async_computation.4 | async-start | bytes 7208960 | tf_op jit(solution)/shard_map/all_gather | solution.py:151
  75.7 331.4 %reduce-scatter.5.cloned.1.call-start = ((), (), s32[]{:S(2)}) async-start(), calls=%async_computation.5 | async-start | bytes 655360 | tf_op jit(solution)/shard_map/reduce_scatter | solution.py:183
  100.8 183.1 %copy-start.5 = (bf16[3,1408]{1,0:T(4,128)(2,1)S(1)}, bf16[3,1408]{1,0:T(4,128)(2,1)}, u32[]{:S(2)}) copy-start(bf16[3,1408]{1,0:T(4,128)(2,1)} %param.31) | copy-start | bytes 25348
  100.8 183.1 %copy-start.6 = (bf16[3,1408]{1,0:T(4,128)(2,1)S(1)}, bf16[3,1408]{1,0:T(4,128)(2,1)}, u32[]{:S(2)}) copy-start(bf16[3,1408]{1,0:T(4,128)(2,1)} %param.30) | copy-start | bytes 25348
  281.3 2.7 collective-permute-start
  282.6 6.0 %collective-permute-start.1 = (bf16[1,2816]{1,0:T(2,128)(2,1)S(1)}, bf16[1,2816]{1,0:T(2,128)(2,1)S(1)}, u32[]{:S(2)}, u32[]{:S(2)}) collective-permute-start(bf16[1,2816]{1,0:T(2,128)(2,1)S(1)} %get-tuple-element.315), channel_id=1, source_target_pairs={{4,0},{8,4},{12,8},{5,1},{9,5},{13,9},{6,2},{10,6},{14,10},{7,3},{... | collective-permute-start | bytes 16904 | tf_op jit(solution)/shard_map/ppermute | solution.py:38
Sparse Core Ops, SparseCore 0:
  72.0 20.8 reduce-scatter.2
  387.2 19.8 reduce-scatter.4
Sparse Core Ops, SparseCore 1:
  75.2 200.1 all-gather.6
  276.8 104.8 all-gather.8
where the time goes:
time: 417 us; the launch traced here: 416 us
  waiting for transfers between devices  309 us (74%)
  blocking collectives  58.9 us (14%)
  matrix products  16.7 us (4%)
  between operations  15.2 us (4%)
  other arithmetic  9.4 us (2%)
    all_gather x1, waiting for transfers between devices, shards(): lax.all_gather(pair_local, 'sp', axis=0, tiled=True)  175 us
    all_gather x1, waiting for transfers between devices, shards(): lax.all_gather(down_weight, 'sp', axis=0, tiled=True)  92.5 us
    all_gather x4, blocking collectives, prefix(): pieces = jax.tree.map(lambda part: lax.all_gather(part, axis), value)  52.3 us
    reduce_scatter x1, waiting for transfers between devices, shards(): lax.psum_scatter(lax.dot_general(picked, down_full, (((1,), (1,)), ((), (...  20 us
    reduce_scatter x1, waiting for transfers between devices, shards(): lax.psum_scatter(jnp.dot(picked, out_weight, preferred_element_type=jnp.f...  17.1 us
  transfers between devices with their start and end apart: 6, of which 5 were waited for; matrix products, arithmetic and copies ran while one was open for 3% of the time, Pallas kernels for 0%

commit v1 on v0

--- a/solution.py
+++ b/solution.py
@@ -147,7 +147,9 @@
     combined = group_norm(ahead_out) * head_gain[0] + group_norm(behind_out) * head_gain[1]
     mixed_heads = (jax.nn.silu(gate_rows.astype(jnp.float32)) * combined).astype(jnp.bfloat16)
     gathered = (
-        lax.all_gather(pair_local, "sp", axis=0, tiled=True),
+        jnp.concatenate(
+            lax.all_to_all(jnp.stack([pair_local] * lax.axis_size("sp")), "sp", 0, 0), axis=0
+        ),
         lax.all_gather(down_weight, "sp", axis=0, tiled=True),
     )
     pair_full, down_full = gathered

time: 417 us -> 469 us (1.12)
  blocking collectives: 58.9 us -> 299 us
  waiting for transfers between devices: 309 us -> 108 us
  starting transfers between devices: 2.71 us -> 11.2 us
  local copies, waits for them, and re-layouts: 3.67 us -> 8.91 us
    all_gather x4, blocking collectives: 52.3 us -> 293 us  [prefix(): pieces = jax.tree.map(lambda part: lax.all_gather(part, axis), value)]
    all_gather x1 -> x0, waiting for transfers between devices: 175 us -> none  [shards(): lax.all_gather(pair_local, 'sp', axis=0, tiled=True)]
    all_gather x1, waiting for transfers between devices: 92.5 us -> 61.3 us  [shards(): lax.all_gather(down_weight, 'sp', axis=0, tiled=True)]
    another operation x1 -> x2, local copies, waits for them, and re-layouts: 0.18 us -> 7.09 us  [the longest x1 6.91 us: shards(): jnp.stack([pair_local] * lax.axis_size('sp'))]
    all_to_all x0 -> x1, starting transfers between devices: none -> 6.48 us  [shards(): lax.all_to_all(jnp.stack([pair_local] * lax.axis_size('sp')), 'sp', 0, 0)]
where the time goes in v1:
time: 469 us; the launch traced here: 468 us
  blocking collectives  299 us (64%)
  waiting for transfers between devices  108 us (23%)
  matrix products  15.9 us (3%)
  between operations  15.2 us (3%)
  starting transfers between devices  11.2 us (2%)
  other arithmetic  9.15 us (2%)
  local copies, waits for them, and re-layouts  8.91 us (2%)
    all_gather x4, blocking collectives, prefix(): pieces = jax.tree.map(lambda part: lax.all_gather(part, axis), value)  293 us
    all_gather x1, waiting for transfers between devices, shards(): lax.all_gather(down_weight, 'sp', axis=0, tiled=True)  61.3 us
    reduce_scatter x1, waiting for transfers between devices, shards(): lax.psum_scatter(lax.dot_general(picked, down_full, (((1,), (1,)), ((), (...  20.1 us
    reduce_scatter x1, waiting for transfers between devices, shards(): lax.psum_scatter(jnp.dot(picked, out_weight, preferred_element_type=jnp.f...  19.8 us
  transfers between devices with their start and end apart: 6, of which 5 were waited for; matrix products, arithmetic and copies ran while one was open for 3% of the time, Pallas kernels for 0%

profile of v1, /device:TPU:0, one launch (start us, length us, event | category | flops | bytes accessed | tf_op | source)
XLA Modules:
  0.0 468.4 jit_solution(864635782819887003)
XLA Ops:
  7.4 3.7 pad_maximum_fusion
  11.1 6.9 %stack.2 = bf16[4,512,2816]{2,1,0:T(8,128)(2,1)} broadcast(bf16[512,2816]{1,0:T(8,128)(2,1)} %pad_maximum_fusion), dimensions={1,2} | broadcast | bytes 14417920 | tf_op jit(solution)/shard_map/stack | solution.py:151
  18.0 6.5 %all-to-all-start = ((bf16[4,512,2816]{2,1,0:T(8,128)(2,1)}), bf16[4,512,2816]{2,1,0:T(8,128)(2,1)}, u32[]{:S(2)}, u32[]{:S(2)}) async-start(bf16[4,512,2816]{2,1,0:T(8,128)(2,1)} %stack.2), calls=%async_computation.1 | async-start | bytes 23068672 | tf_op jit(solution)/shard_map/all_to_all | solution.py:151
  24.5 0.3 reduce_window_sum.17
  24.8 0.2 exponential_reduce_fusion.1
  25.0 192.1 %all-gather.2 = f32[4,1,2]{2,1,0:T(1,128)S(1)} all-gather(f32[1,1,2]{2,1,0:T(1,128)S(1)} %bitcast.180), channel_id=1, replica_groups=mesh['grp'=2,'sp'=4,'tp'=4] {'sp'}, dimensions={0}, use_global_device_ids=true | all-gather | bytes 40 | tf_op jit(solution)/shard_map/all_gather | solution.py:15
  217.1 0.1 rev.23
  217.2 0.3 reduce_window_sum.18
  217.5 0.2 exponential_reduce_fusion
  217.7 70.3 %all-gather.3 = f32[4,1,2]{2,1,0:T(1,128)S(1)} all-gather(f32[1,1,2]{2,1,0:T(1,128)S(1)} %bitcast.181), channel_id=1, replica_groups=mesh['grp'=2,'sp'=4,'tp'=4] {'sp'}, dimensions={0}, use_global_device_ids=true | all-gather | bytes 40 | tf_op jit(solution)/shard_map/all_gather | solution.py:15
  288.0 0.1 copy.89
  288.1 0.2 reverse.3
  288.4 0.1 rev.24
  288.5 0.2 slice_reduce_fusion
  288.7 0.3 convolution_add_fusion.1
  289.0 14.9 %all-gather.1 = f32[8,128,128]{2,1,0:T(8,128)S(1)} all-gather(f32[2,128,128]{2,1,0:T(8,128)S(1)} %convolution_add_fusion.1), channel_id=3, replica_groups=mesh['grp'=2,'sp'=4,'tp'=4] {'sp'}, dimensions={0}, use_global_device_ids=true | all-gather | bytes 655360 | tf_op jit(solution)/shard_map/all_gather | solution.py:15
  304.0 0.1 copy.75
  304.1 0.1 rev.25
  304.2 0.1 copy.76
  304.3 0.1 rev.22
  304.4 0.4 fusion.11
  304.8 0.3 fusion.30
  305.1 0.4 while.19
  305.2 0.1 fusion.85
  305.3 0.1 fusion.85
  305.4 0.1 fusion.85
  305.5 0.3 convolution_bitcast_fusion
  305.8 0.4 fusion.7
  306.2 0.1 rev.27
  306.3 0.1 reduce_sum.47
  306.4 0.2 multiply_reduce_fusion
  306.6 0.1 subtract_multiply_fusion
  306.8 0.1 copy.79
  306.9 0.1 copy.58
  307.0 0.2 slice_reduce_fusion.1
  307.2 0.3 fusion.9
  307.6 0.2 convolution_add_fusion
  307.8 15.5 %all-gather = f32[8,128,128]{2,1,0:T(8,128)S(1)} all-gather(f32[2,128,128]{2,1,0:T(8,128)S(1)} %convolution_add_fusion), channel_id=2, replica_groups=mesh['grp'=2,'sp'=4,'tp'=4] {'sp'}, dimensions={0}, use_global_device_ids=true | all-gather | bytes 655360 | tf_op jit(solution)/shard_map/all_gather | solution.py:15
  323.3 0.5 fusion.33
  323.8 0.4 while.18
  323.8 0.1 fusion.84
  324.0 0.1 fusion.84
  324.1 0.1 fusion.84
  324.2 0.4 convolution_bitcast_fusion.3
  324.6 0.3 fusion.62
  325.0 0.1 fusion.28
  325.2 1.1 convolution_convert_fusion.1
  326.4 0.5 all-gather.6.cloned.1.call-update
  327.0 19.8 %reduce-scatter.3.cloned.1.call-done = bf16[32,2048]{1,0:T(8,128)(2,1)} async-done(((bf16[128,2048]{1,0:T(8,128)(2,1)}), bf16[32,2048]{1,0:T(8,128)(2,1)}) %reduce-scatter.3.cloned.1.call-update) | async-done | bytes 131088 | tf_op jit(solution)/shard_map/reduce_scatter | solution.py:159
  346.8 1.0 add_convert_fusion
  347.8 0.1 fusion.15
  348.0 0.1 fusion.17
  348.1 6.6 %all_gather.26 = bf16[128,2048]{1,0:T(8,128)(2,1)S(1)} all-gather(bf16[32,2048]{1,0:T(8,128)(2,1)S(1)} %fusion.17), channel_id=1, replica_groups=mesh['grp'=2,'sp'=4,'tp'=4] {'tp'}, dimensions={0}, use_global_device_ids=true | all-gather | bytes 655360 | tf_op jit(solution)/shard_map/all_gather | solution.py:171
  354.7 6.0 %convolution_convert_fusion = bf16[128,2816]{1,0:T(8,128)(2,1)S(1)} fusion(bf16[128,2048]{1,0:T(8,128)(2,1)S(1)} %all_gather.26, bf16[2048,2816]{1,0:T(8,128)(2,1)} %bitcast.30), kind=kOutput, calls=%fused_computation.6 | convolution fusion | flops 1476755456 | bytes 12779520 | tf_op jit(solution)/shard_map/dot_general | solution.py:170
  360.7 3.4 collective-permute-start
  364.1 1.3 collective-permute-start.1
  365.4 0.1 convert_reduce_fusion.1
  365.5 0.1 collective-permute-done
  365.7 6.4 %collective-permute-done.1 = bf16[1,2816]{1,0:T(2,128)(2,1)S(1)} collective-permute-done((bf16[1,2816]{1,0:T(2,128)(2,1)S(1)}, bf16[1,2816]{1,0:T(2,128)(2,1)S(1)}, u32[]{:S(2)}, u32[]{:S(2)}) %collective-permute-start.1) | collective-permute-done | bytes 5664 | tf_op jit(solution)/shard_map/ppermute | solution.py:38
  372.0 0.5 multiply_add_fusion
  372.5 61.3 %all-gather.6.cloned.1.call-done = bf16[2048,1408]{1,0:T(8,128)(2,1)} async-done(((bf16[512,1408]{1,0:T(8,128)(2,1)}), bf16[2048,1408]{1,0:T(8,128)(2,1)}) %all-gather.6.cloned.1.call-update) | async-done | bytes 5767184 | tf_op jit(solution)/shard_map/all_gather | solution.py:153
  433.9 5.4 %convolution_convert_fusion.2 = bf16[128,2048]{1,0:T(8,128)(2,1)} fusion(bf16[2048,1408]{1,0:T(8,128)(2,1)} %all-gather.6.cloned.1.call-done, f32[128,2816]{1,0:T(8,128)S(1)} %multiply_add_fusion), kind=kOutput, calls=%fused_computation.9 | convolution fusion | flops 739540992 | bytes 7733248 | tf_op jit(solution)/shard_map/dot_general | solution.py:186
  439.3 20.1 %reduce-scatter.5.cloned.1.call-done = bf16[32,2048]{1,0:T(8,128)(2,1)} async-done(((bf16[128,2048]{1,0:T(8,128)(2,1)}), bf16[32,2048]{1,0:T(8,128)(2,1)}) %reduce-scatter.5.cloned.1.call-update) | async-done | bytes 131088 | tf_op jit(solution)/shard_map/reduce_scatter | solution.py:185
  459.4 1.6 fusion.18
  (53 shorter events, 0.6 us)
Async XLA Ops:
  7.4 317.8 %copy-start = (bf16[256,2048]{1,0:T(8,128)(2,1)S(1)}, bf16[256,2048]{1,0:T(8,128)(2,1)}, u32[]{:S(2)}) copy-start(bf16[256,2048]{1,0:T(8,128)(2,1)} %param.24) | copy-start | bytes 3145732
  18.0 6.5 %copy-start.8 = (f32[2,2,128]{2,1,0:T(2,128)S(1)}, f32[2,2,128]{2,1,0:T(2,128)}, u32[]{:S(2)}) copy-start(f32[2,2,128]{2,1,0:T(2,128)} %param.22) | copy-start | bytes 6148
  18.0 270.0 %copy-start.3 = (bf16[128,256]{1,0:T(8,128)(2,1)S(1)}, bf16[128,256]{1,0:T(8,128)(2,1)}, u32[]{:S(2)}) copy-start(bf16[128,256]{1,0:T(8,128)(2,1)} %param.19) | copy-start | bytes 196612
  18.0 270.3 %copy-start.2 = (bf16[128,256]{1,0:T(8,128)(2,1)S(1)}, bf16[128,256]{1,0:T(8,128)(2,1)}, u32[]{:S(2)}) copy-start(bf16[128,256]{1,0:T(8,128)(2,1)} %param.20) | copy-start | bytes 196612
  18.0 336.6 %all-to-all-start = ((bf16[4,512,2816]{2,1,0:T(8,128)(2,1)}), bf16[4,512,2816]{2,1,0:T(8,128)(2,1)}, u32[]{:S(2)}, u32[]{:S(2)}) async-start(bf16[4,512,2816]{2,1,0:T(8,128)(2,1)} %stack.2), calls=%async_computation.1 | async-start | bytes 23068672 | tf_op jit(solution)/shard_map/all_to_all | solution.py:151
  24.5 322.3 %reduce-scatter.3.cloned.1.call-start = ((), (), s32[]{:S(2)}) async-start(), calls=%async_computation.3 | async-start | bytes 655360 | tf_op jit(solution)/shard_map/reduce_scatter | solution.py:159
  288.1 16.2 %copy-start.1 = (bf16[128,256]{1,0:T(8,128)(2,1)S(1)}, bf16[128,256]{1,0:T(8,128)(2,1)}, u32[]{:S(2)}) copy-start(bf16[128,256]{1,0:T(8,128)(2,1)} %param.18) | copy-start | bytes 196612
  305.5 1.4 copy-start.4
  323.8 1.2 copy-start.9
  325.2 1.8 copy-start.7
  326.3 107.5 %all-gather.6.cloned.1.call-start = ((), (), s32[]{:S(2)}) async-start(), calls=%async_computation.4 | async-start | bytes 7208960 | tf_op jit(solution)/shard_map/all_gather | solution.py:153
  326.9 132.4 %reduce-scatter.5.cloned.1.call-start = ((), (), s32[]{:S(2)}) async-start(), calls=%async_computation.5 | async-start | bytes 655360 | tf_op jit(solution)/shard_map/reduce_scatter | solution.py:185
  354.7 10.8 %copy-start.5 = (bf16[3,1408]{1,0:T(4,128)(2,1)S(1)}, bf16[3,1408]{1,0:T(4,128)(2,1)}, u32[]{:S(2)}) copy-start(bf16[3,1408]{1,0:T(4,128)(2,1)} %param.31) | copy-start | bytes 25348
  354.7 10.8 %copy-start.6 = (bf16[3,1408]{1,0:T(4,128)(2,1)S(1)}, bf16[3,1408]{1,0:T(4,128)(2,1)}, u32[]{:S(2)}) copy-start(bf16[3,1408]{1,0:T(4,128)(2,1)} %param.30) | copy-start | bytes 25348
  360.7 4.9 %collective-permute-start = (bf16[1,2816]{1,0:T(2,128)(2,1)S(1)}, bf16[1,2816]{1,0:T(2,128)(2,1)S(1)}, u32[]{:S(2)}, u32[]{:S(2)}) collective-permute-start(bf16[1,2816]{1,0:T(2,128)(2,1)S(1)} %get-tuple-element.314), channel_id=1, source_target_pairs={{0,4},{4,8},{8,12},{1,5},{5,9},{9,13},{2,6},{6,10},{10,14},{3,7},{... | collective-permute-start | bytes 16904 | tf_op jit(solution)/shard_map/ppermute | solution.py:37
  364.1 7.9 %collective-permute-start.1 = (bf16[1,2816]{1,0:T(2,128)(2,1)S(1)}, bf16[1,2816]{1,0:T(2,128)(2,1)S(1)}, u32[]{:S(2)}, u32[]{:S(2)}) collective-permute-start(bf16[1,2816]{1,0:T(2,128)(2,1)S(1)} %get-tuple-element.315), channel_id=1, source_target_pairs={{4,0},{8,4},{12,8},{5,1},{9,5},{13,9},{6,2},{10,6},{14,10},{7,3},{... | collective-permute-start | bytes 16904 | tf_op jit(solution)/shard_map/ppermute | solution.py:38
Sparse Core Ops, SparseCore 0:
  326.5 20.2 reduce-scatter.2
  439.4 19.9 reduce-scatter.4
Sparse Core Ops, SparseCore 1:
  328.4 105.4 all-gather.5
